TPU v7x, 32 devices: a whole 2x2x4 slice. The times are simulated.
32 devices in a mesh: sp: 16 (over z, y, core), tp: 2 (over x).
Axes of the slice: x: 2, y: 2, z: 4, core: 2. Of those that a mesh axis runs over, the one named last changes fastest.
Arguments:
- glu_value: bfloat16 [8192, 1024], P('sp', 'tp'), may hold values from -6 to 6
- glu_gate: bfloat16 [8192, 1024], P('sp', 'tp'), may hold values from -8 to 8
- conv_taps: float32 [31, 1024], P(None, 'tp'), may hold values from -1 to 1
- channel_norm_gain: float32 [1024], P('tp'), may hold values from 0.1 to 1.9
- channel_norm_bias: float32 [1024], P('tp'), may hold values from -3 to 3
- out_proj: bfloat16 [1024, 2048], P('tp'), may hold values from -0.1875 to 0.1875
- out_grad: bfloat16 [8192, 2048], P('sp'), may hold values from -6 to 6
Outputs:
- grad_value: bfloat16 [8192, 1024], P('sp', 'tp')
- grad_gate: bfloat16 [8192, 1024], P('sp', 'tp')
- grad_taps: float32 [31, 1024], P(None, 'tp')
- norm_gain_gradient: float32 [1024], P('tp')
- grad_bias: float32 [1024], P('tp')
- grad_proj: float32 [2048, 1024], P('sp', 'tp')
All inputs are finite; a program needn't handle non-finite values.
Results may differ from a plain program's by a relative error of at most 0.0049.
Values may be sent and summed in bfloat16 or wider, within the bound.
A program may use at most 64 MiB of HBM per device.

v0:
```python
import jax
import jax.numpy as jnp
from jax import lax
from jax.sharding import PartitionSpec as P

CONV_CHANNELS = 1024
TAPS = 31


def passed_along(shard, axis, by):
    size = lax.axis_size(axis)
    pairs = [(i, i + by) for i in range(size) if 0 <= i + by < size]
    return lax.ppermute(shard, axis, pairs)


def on_device(
    glu_value, glu_gate, conv_taps, channel_norm_gain, channel_norm_bias, out_proj, out_grad
):
    rows, width = glu_value.shape
    value = glu_value.astype(jnp.float32)
    sig_gate = jax.nn.sigmoid(glu_gate.astype(jnp.float32))
    gated = (value * sig_gate).astype(jnp.bfloat16)
    before = passed_along(gated[rows - (TAPS - 1) :], "sp", 1)
    padded = jnp.concatenate([before, gated], axis=0).astype(jnp.float32)
    conv_output = jnp.zeros((rows, width), jnp.float32)
    for k in range(TAPS):
        conv_output = conv_output + conv_taps[k][None, :] * padded[k : k + rows]
    total, squares = lax.psum(
        (jnp.sum(conv_output, axis=1), jnp.sum(conv_output * conv_output, axis=1)), "tp"
    )
    channel_mean = (total / CONV_CHANNELS)[:, None]
    var = (squares / CONV_CHANNELS)[:, None] - channel_mean * channel_mean
    inverse_deviation = lax.rsqrt(var + 1e-05)
    centered_standardized = (conv_output - channel_mean) * inverse_deviation
    normalized_rows = (
        centered_standardized * channel_norm_gain[None, :] + channel_norm_bias[None, :]
    )
    sig_norm = jax.nn.sigmoid(normalized_rows)
    act = (normalized_rows * sig_norm).astype(jnp.bfloat16)
    grad_act = lax.dot_general(
        out_grad, out_proj, (((1,), (1,)), ((), ())), preferred_element_type=jnp.float32
    )
    grad_proj = lax.psum_scatter(
        lax.dot_general(
            out_grad, act, (((0,), (0,)), ((), ())), preferred_element_type=jnp.float32
        ),
        "sp",
        scatter_dimension=0,
        tiled=True,
    )
    normalized_gradient = grad_act * sig_norm * (1.0 + normalized_rows * (1.0 - sig_norm))
    scaled_rows = normalized_gradient * channel_norm_gain[None, :]
    first_term, second_term = lax.psum(
        (jnp.sum(scaled_rows, axis=1), jnp.sum(scaled_rows * centered_standardized, axis=1)), "tp"
    )
    conv_output_gradient = inverse_deviation * (
        scaled_rows
        - (first_term / CONV_CHANNELS)[:, None]
        - centered_standardized * (second_term / CONV_CHANNELS)[:, None]
    )
    taps_local = jnp.stack(
        [jnp.sum(conv_output_gradient * padded[k : k + rows], axis=0) for k in range(TAPS)], axis=0
    )
    packed = jnp.concatenate(
        [
            taps_local,
            jnp.sum(normalized_gradient * centered_standardized, axis=0)[None, :],
            jnp.sum(normalized_gradient, axis=0)[None, :],
        ],
        axis=0,
    )
    share = lax.psum_scatter(packed, "sp", scatter_dimension=1, tiled=True)
    summed = lax.all_gather(share, "sp", axis=1, tiled=True)
    ahead = passed_along(conv_output_gradient[: TAPS - 1], "sp", -1)
    after = jnp.concatenate([conv_output_gradient, ahead], axis=0)
    grad_gated = jnp.zeros((rows, width), jnp.float32)
    for k in range(TAPS):
        grad_gated = grad_gated + conv_taps[k][None, :] * after[TAPS - 1 - k : TAPS - 1 - k + rows]
    grad_value = (grad_gated * sig_gate).astype(jnp.bfloat16)
    grad_gate = (grad_gated * value * sig_gate * (1.0 - sig_gate)).astype(jnp.bfloat16)
    return (grad_value, grad_gate, summed[:TAPS], summed[TAPS], summed[TAPS + 1], grad_proj)


def solution(mesh):
    return jax.shard_map(
        on_device,
        mesh=mesh,
        in_specs=(
            P("sp", "tp"),
            P("sp", "tp"),
            P(None, "tp"),
            P("tp"),
            P("tp"),
            P("tp", None),
            P("sp", None),
        ),
        out_specs=(P("sp", "tp"), P("sp", "tp"), P(None, "tp"), P("tp"), P("tp"), P("sp", "tp")),
        check_vma=False,
    )
```

profile of v0, /device:TPU:0, one launch (start us, length us, event | category | flops | bytes accessed | tf_op | source)
XLA Modules:
  0.0 184.4 jit_solution(906869488730801096)
XLA Ops:
  7.2 0.0 copy-start
  7.2 0.0 reduce-scatter.7.cloned.1.call-start
  7.2 1.6 fusion.1
  8.9 2.4 %collective-permute-start = (bf16[30,512]{1,0:T(8,128)(2,1)S(1)}, bf16[30,512]{1,0:T(8,128)(2,1)S(1)}, u32[]{:S(2)}, u32[]{:S(2)}) collective-permute-start(bf16[30,512]{1,0:T(8,128)(2,1)S(1)} %slice.450), channel_id=1, source_target_pairs={{0,2},{2,4},{4,6},{6,8},{8,10},{10,12},{12,14},{14,16},{16,18},{18... | collective-permute-start | bytes 92168 | tf_op jit(solution)/shard_map/ppermute | solution.py:13
  11.3 1.1 fusion.101
  12.4 1.0 fusion.102
  13.5 0.0 collective-permute-done
  13.5 0.2 maximum_convert_fusion
  13.6 0.0 copy-start.4
  13.6 0.0 copy-start.5
  13.7 5.7 %multiply_reduce_fusion.33 = (f32[512]{0:T(512)S(1)}, f32[512]{0:T(512)S(1)}, f32[512,512]{1,0:T(8,128)}) fusion(f32[542,512]{1,0:T(8,128)S(1)} %maximum_convert_fusion, f32[512]{0:T(512)S(1)} %bitcast.132, f32[512]{0:T(512)S(1)} %bitcast.134, f32[512]{0:T(512)S(1)} %bitcast.76, f32[512]{0:T(512)S(1)} %bitcast.78, f32[512]{0:T(512)S(1)} %bitcast.80, ...), kind=kLoop, calls=%fused_computation.184 | loop fusion | flops 16776192 | bytes 33622016 | tf_op jit(solution)/shard_map/reduce_sum | solution.py:29
  19.4 5.2 %all-reduce.1 = (f32[512]{0:T(512)S(1)}, f32[512]{0:T(512)S(1)}) all-reduce(f32[512]{0:T(512)S(1)} %get-tuple-element.60, f32[512]{0:T(512)S(1)} %get-tuple-element.59), channel_id=1, replica_groups=mesh['sp'=16,'tp'=2] {'tp'}, use_global_device_ids=true, to_apply=%region_3.0 | all-reduce | flops 1024 | bytes 8192 | tf_op jit(solution)/shard_map/psum | solution.py:28
  24.6 0.0 copy-done
  24.6 0.0 copy-done.4
  24.6 0.0 copy-done.5
  24.6 4.6 %multiply_reduce_fusion = (f32[512]{0:T(512)S(1)}, f32[512]{0:T(512)S(1)}, f32[512]{0:T(512)S(1)}, f32[512]{0:T(512)S(1)}, f32[512,512]{1,0:T(8,128)}) fusion(f32[512,512]{1,0:T(8,128)} %get-tuple-element.70, f32[512]{0:T(512)S(1)} %get-tuple-element.103, f32[512]{0:T(512)S(1)} %get-tuple-element.102, f32[512]{0:T(512)S(1)} %copy-done.4, ...), kind=kOutput, calls=%fused_computation.146 | convolution fusion | flops 1078720512 | bytes 6307840 | tf_op jit(solution)/shard_map/dot_general | solution.py:40
  29.2 4.9 %all-reduce = (f32[512]{0:T(512)S(1)}, f32[512]{0:T(512)S(1)}) all-reduce(f32[512]{0:T(512)S(1)} %get-tuple-element.56, f32[512]{0:T(512)S(1)} %get-tuple-element.57), channel_id=1, replica_groups=mesh['sp'=16,'tp'=2] {'tp'}, use_global_device_ids=true, to_apply=%region_7.0 | all-reduce | flops 1024 | bytes 8192 | tf_op jit(solution)/shard_map/psum | solution.py:53
  34.1 4.2 %multiply_reduce_fusion.1 = (f32[512]{0:T(512)S(1)}, f32[512]{0:T(512)S(1)}, f32[512]{0:T(512)S(1)}, f32[512]{0:T(512)S(1)}, f32[512]{0:T(512)S(1)}, /*index=5*/...) fusion(f32[542,512]{1,0:T(8,128)S(1)} %maximum_convert_fusion, ...), kind=kLoop, calls=%fused_computation.147 | loop fusion | flops 11262976 | bytes 22067200 | tf_op jit(solution)/shard_map/reduce_sum | solution.py:62
  38.3 0.0 copy-start.1
  38.3 1.7 multiply_reduce_fusion.19
  40.0 0.0 copy-done.1
  40.0 0.2 concatenate.11
  40.2 0.8 copy.20
  41.0 0.0 reduce-scatter.7.cloned.1.call-update
  41.1 0.0 reduce-scatter.5.cloned.1.call-start
  41.1 4.6 %convolution_bitcast_fusion = f32[2048,512]{0,1:T(8,128)} fusion(bf16[512,2048]{1,0:T(8,128)(2,1)S(1)} %copy-done, f32[512,512]{1,0:T(8,128)} %get-tuple-element.70, f32[512]{0:T(512)S(1)} %copy-done.5, f32[512]{0:T(512)S(1)} %copy-done.4, f32[512]{0:T(512)S(1)} %get-tuple-element.103, f32[512]{0:T(512)S(1)} %get-tuple-element.102), kind=kOutput, calls=%fused_computation.29 | convolution fusion | flops 1076101120 | bytes 7348224 | tf_op jit(solution)/shard_map/dot_general | solution.py:44
  45.7 0.0 copy-start.2
  45.7 0.0 reduce-scatter.5.cloned.1.call-update
  45.8 1.2 copy-done.2
  47.0 0.0 copy-start.3
  47.0 1.4 collective-permute-start.1
  48.4 1.8 %collective-permute-done.1 = f32[30,512]{1,0:T(8,128)S(1)} collective-permute-done((f32[30,512]{1,0:T(8,128)S(1)}, f32[30,512]{1,0:T(8,128)S(1)}, u32[]{:S(2)}, u32[]{:S(2)}) %collective-permute-start.1) | collective-permute-done | bytes 61472 | tf_op jit(solution)/shard_map/ppermute | solution.py:13
  50.2 7.0 %fusion.4 = (bf16[512,512]{1,0:T(8,128)(2,1)}, f32[512,512]{1,0:T(8,128)S(1)}) fusion(bf16[512,512]{1,0:T(8,128)(2,1)} %param.7, bf16[512,512]{1,0:T(8,128)(2,1)} %param.8, f32[512,512]{1,0:T(8,128)S(1)} %copy-done.2, f32[512]{0:T(512)S(1)} %bitcast.133, f32[30,512]{1,0:T(8,128)S(1)} %collective-permute-done.1, f32[512]{0:T(512)S(1)} %bitcast.135, ...), kind=kLoop, calls=%fused_computation.37 | loop fusion | flops 26476544 | bytes 3794944 | tf_op jit(solution)/shard_map/convert_element_type | solution.py:80
  57.2 0.0 copy-done.3
  57.2 1.1 multiply_convert_fusion.1
  58.3 41.8 %reduce-scatter.7.cloned.1.call-done = f32[32,33]{1,0:T(8,128)} async-done(((f32[512,33]{1,0:T(8,128)}), f32[32,33]{1,0:T(8,128)}) %reduce-scatter.7.cloned.1.call-update) | async-done | bytes 4240
  100.1 20.3 %all_gather.3 = f32[33,512]{0,1:T(8,128)S(1)} all-gather(f32[33,32]{0,1:T(8,128)} %bitcast.136), channel_id=1, replica_groups=mesh['sp'=16,'tp'=2] {'sp'}, dimensions={1}, use_global_device_ids=true | all-gather | bytes 71808 | tf_op jit(solution)/shard_map/all_gather | solution.py:73
  120.4 0.7 copy.18
  121.2 1.0 slice_reduce_fusion
  122.1 53.6 %reduce-scatter.5.cloned.1.call-done = f32[128,512]{0,1:T(8,128)} async-done(((f32[2048,512]{0,1:T(8,128)}), f32[128,512]{0,1:T(8,128)}) %reduce-scatter.5.cloned.1.call-update) | async-done | bytes 262160 | tf_op jit(solution)/shard_map/reduce_scatter | solution.py:43
  175.8 1.8 copy.19
  (4 shorter events, 0.0 us)
Async XLA Ops:
  7.2 17.4 %copy-start = (bf16[512,2048]{1,0:T(8,128)(2,1)S(1)}, bf16[512,2048]{1,0:T(8,128)(2,1)}, u32[]{:S(2)}) copy-start(bf16[512,2048]{1,0:T(8,128)(2,1)} %param.13) | copy-start | bytes 6291460
  7.2 92.9 %reduce-scatter.7.cloned.1.call-start = ((), (), s32[]{:S(2)}) async-start(), calls=%async_computation.3 | async-start | bytes 278528
  8.9 4.6 %collective-permute-start = (bf16[30,512]{1,0:T(8,128)(2,1)S(1)}, bf16[30,512]{1,0:T(8,128)(2,1)S(1)}, u32[]{:S(2)}, u32[]{:S(2)}) collective-permute-start(bf16[30,512]{1,0:T(8,128)(2,1)S(1)} %slice.450), channel_id=1, source_target_pairs={{0,2},{2,4},{4,6},{6,8},{8,10},{10,12},{12,14},{14,16},{16,18},{18... | collective-permute-start | bytes 92168 | tf_op jit(solution)/shard_map/ppermute | solution.py:13
  13.6 11.0 %copy-start.4 = (f32[512]{0:T(512)S(1)}, f32[512]{0:T(512)}, u32[]{:S(2)}) copy-start(f32[512]{0:T(512)} %param.10) | copy-start | bytes 6148
  13.6 11.0 %copy-start.5 = (f32[512]{0:T(512)S(1)}, f32[512]{0:T(512)}, u32[]{:S(2)}) copy-start(f32[512]{0:T(512)} %param.11) | copy-start | bytes 6148
  38.3 1.7 copy-start.1
  41.1 134.7 %reduce-scatter.5.cloned.1.call-start = ((), (), s32[]{:S(2)}) async-start(), calls=%async_computation.2 | async-start | bytes 4456448 | tf_op jit(solution)/shard_map/reduce_scatter | solution.py:43
  45.7 1.2 copy-start.2
  47.0 10.3 %copy-start.3 = (bf16[512,512]{1,0:T(8,128)(2,1)S(1)}, bf16[512,512]{1,0:T(8,128)(2,1)}, u32[]{:S(2)}) copy-start(bf16[512,512]{1,0:T(8,128)(2,1)} %param.8) | copy-start | bytes 1572868
  47.0 3.3 %collective-permute-start.1 = (f32[30,512]{1,0:T(8,128)S(1)}, f32[30,512]{1,0:T(8,128)S(1)}, u32[]{:S(2)}, u32[]{:S(2)}) collective-permute-start(f32[30,512]{1,0:T(8,128)S(1)} %slice.482), channel_id=1, source_target_pairs={{2,0},{4,2},{6,4},{8,6},{10,8},{12,10},{14,12},{16,14},{18,16},{20... | collective-permute-start | bytes 184328 | tf_op jit(solution)/shard_map/ppermute | solution.py:13
Sparse Core Ops, SparseCore 0:
  41.2 58.8 reduce-scatter.6
  103.9 71.7 reduce-scatter.4
where the time goes:
time: 185 us; the launch traced here: 184 us
  waiting for transfers between devices  97.3 us (53%)
  blocking collectives  30.4 us (16%)
  other arithmetic  21.5 us (12%)
  between operations  14.2 us (8%)
  matrix products  9.17 us (5%)
  local copies, waits for them, and re-layouts  7.9 us (4%)
  starting transfers between devices  3.9 us (2%)
    reduce_scatter x1, waiting for transfers between devices, on_device(): lax.psum_scatter(lax.dot_general(out_grad, act, (((0,), (0,)), ((), ())),...  53.6 us
    unnamed x3, waiting for transfers between devices  41.8 us
    all_gather x1, blocking collectives, on_device(): summed = lax.all_gather(share, 'sp', axis=1, tiled=True)  20.3 us
    convert_element_type x1, other arithmetic, on_device(): (grad_gated * value * sig_gate * (1.0 - sig_gate)).astype(jnp.bfloat16)  6.99 us
    reduce_sum x2, other arithmetic, on_device(): jnp.sum(conv_output_gradient * padded[k:k + rows], axis=0)  5.89 us
    reduce_sum x1, other arithmetic, on_device(): jnp.sum(conv_output * conv_output, axis=1)  5.75 us
    psum x1, blocking collectives, on_device(): lax.psum((jnp.sum(conv_output, axis=1), jnp.sum(conv_output * conv_output...  5.19 us
    psum x1, blocking collectives, on_device(): lax.psum((jnp.sum(scaled_rows, axis=1), jnp.sum(scaled_rows * centered_st...  4.91 us
  transfers between devices with their start and end apart: 4, of which 3 were waited for; matrix products, arithmetic and copies ran while one was open for 9% of the time, Pallas kernels for 0%

commit v1 on v0

v1 whole, which is shorter than its diff:
```python
import functools

import jax
import jax.numpy as jnp
from jax import lax
from jax.experimental import pallas as pl
from jax.experimental.pallas import tpu as pltpu
from jax.sharding import PartitionSpec as P

LANES = 128
HALO = 32
SMALL = 40
MESH = pl.DeviceIdType.MESH
F32, BF16 = jnp.float32, jnp.bfloat16


def kernel(
    n, tp, taps_n,
    value_hbm, gate_hbm, taps_ref, gain_ref, bias_ref, proj_hbm, grad_hbm,
    gv_hbm, gg_hbm, small_hbm, gp_hbm,
    value, gate, proj, grad, gpad, conv, gact, gnorm, gcpad, act,
    full, pair_out, pair_in, ring_out, ring_in,
    halo_out, halo_in, back_out, back_in,
    stage, mean_b, rstd_b, stat_out, stat_in, stat2_out, stat2_in,
    tacc, small, small_in, small_all, small_fin, small_tot,
    gv, gg, gp,
    in_sem, out_sem, halo_sem, back_sem, stat_sem, stat2_sem,
    pair_s, pair_r, ring_s, ring_r, sp_sem, sa_s, sa_r, sf_sem,
):
    rows, width = value.shape
    blocks = width // LANES
    chunks = rows // LANES
    nc = n // 2
    half = blocks // 2
    share = full.shape[1]
    model = grad.shape[1]
    channels = width * tp
    me = lax.axis_index("sp")
    col = lax.axis_index("tp")
    par = lax.rem(me, 2)
    chip = me // 2
    partner = chip * 2 + 1 - par
    nxt = lax.rem(me + 1, n)
    prv = lax.rem(me + n - 1, n)

    loads = [
        pltpu.make_async_copy(s, d, in_sem.at[i])
        for i, (s, d) in enumerate(
            ((value_hbm, value), (gate_hbm, gate), (grad_hbm, grad), (proj_hbm, proj))
        )
    ]
    for c in loads:
        c.start()

    barrier = pltpu.get_barrier_semaphore()

    @pl.loop(1, n)
    def _(i):
        pl.semaphore_signal(
            barrier, inc=1, device_id={"sp": lax.rem(me + i, n)}, device_id_type=MESH
        )

    for t in range(1, tp):
        pl.semaphore_signal(
            barrier, inc=1, device_id={"tp": lax.rem(col + t, tp)}, device_id_type=MESH
        )

    def remote(src, dst, s, r, where):
        return pltpu.make_async_remote_copy(
            src_ref=src, dst_ref=dst, send_sem=s, recv_sem=r,
            device_id=where, device_id_type=MESH,
        )

    def lanes(cb):
        return pl.ds(pl.multiple_of(cb * LANES, LANES), LANES)

    def stat_copy(out, inn, sem, j, t):
        return remote(
            out.at[j], inn.at[j, t - 1], sem.at[0, j, t - 1], sem.at[1, j, t - 1],
            {"tp": lax.rem(col + t, tp)},
        )

    sub = lax.broadcasted_iota(jnp.int32, (8, LANES), 0)

    def send_stats(out, inn, sem, j):
        a = jnp.sum(stage[0].T, axis=0, keepdims=True)
        b = jnp.sum(stage[1].T, axis=0, keepdims=True)
        out[j] = jnp.where(sub == 0, a, b)
        for t in range(1, tp):
            stat_copy(out, inn, sem, j, t).start()

    def recv_stats(out, inn, sem, j):
        total = out[j]
        for t in range(1, tp):
            stat_copy(out, inn, sem, j, t).wait()
            total = total + inn[j, t - 1]
        total = total / channels
        return total[0:1], total[1:2]

    loads[0].wait()
    loads[1].wait()

    def gated_rows(r0, cb, count):
        v = value[pl.ds(r0, count), lanes(cb)].astype(F32)
        s = jax.nn.sigmoid(gate[pl.ds(r0, count), lanes(cb)].astype(F32))
        return (v * s).astype(BF16)

    for cb in range(blocks):
        g = gated_rows(rows - HALO, cb, HALO)
        halo_out[cb] = g
    pl.semaphore_wait(barrier, n - 1 + tp - 1)
    halo = remote(halo_out, halo_in, halo_sem.at[0], halo_sem.at[1], {"sp": nxt})
    halo.start()

    @pl.loop(0, rows // 64)
    def _(i):
        r0 = pl.multiple_of(i * 64, 64)
        for cb in range(blocks):
            gpad[cb, pl.ds(r0 + HALO, 64), :] = gated_rows(r0, cb, 64).astype(F32)

    def tap_row(k, cb):
        return taps_ref[pl.ds(k, 1), lanes(cb)]

    def conv_chunk(j):
        for h in range(LANES // 64):
            r0 = j * LANES + h * 64

            def body(cb, carry):
                s, q = carry
                acc = tap_row(0, cb) * gpad[cb, pl.ds(r0 + 2, 64), :]
                for k in range(1, taps_n):
                    acc = acc + tap_row(k, cb) * gpad[cb, pl.ds(r0 + HALO - taps_n + 1 + k, 64), :]
                conv[cb, pl.ds(r0, 64), :] = acc
                return s + acc, q + acc * acc

            zero = jnp.zeros((64, LANES), F32)
            s, q = lax.fori_loop(0, blocks, body, (zero, zero))
            stage[0, pl.ds(h * 64, 64), :] = s
            stage[1, pl.ds(h * 64, 64), :] = q
        send_stats(stat_out, stat_in, stat_sem, j)

    order = list(range(1, chunks)) + [0]
    for j in order:
        if j == 0:
            halo.wait()
            first = me == 0
            for cb in range(blocks):
                h = halo_in[cb].astype(F32)
                gpad[cb, pl.ds(0, HALO), :] = jnp.where(first, jnp.zeros_like(h), h)
        conv_chunk(j)

    loads[2].wait()
    loads[3].wait()
    for cb in range(blocks):
        gact[cb] = lax.dot_general(
            grad[...], proj[pl.ds(cb * LANES, LANES), :], (((1,), (1,)), ((), ())),
            preferred_element_type=F32,
        )

    tacc[...] = jnp.zeros_like(tacc)

    def norm_chunk(j):
        mean, sq = recv_stats(stat_out, stat_in, stat_sem, j)
        rstd = lax.rsqrt(sq - mean * mean + 1e-05)
        mean_b[...] = jnp.broadcast_to(mean, (LANES, LANES)).T
        rstd_b[pl.ds(j * LANES, LANES), :] = jnp.broadcast_to(rstd, (LANES, LANES)).T

        @pl.loop(0, LANES // 32)
        def _(h):
            l0 = pl.multiple_of(h * 32, 32)
            r0 = pl.multiple_of(j * LANES + l0, 32)
            m = mean_b[pl.ds(l0, 32), :]
            rs = rstd_b[pl.ds(r0, 32), :]
            s1 = jnp.zeros((32, LANES), F32)
            s2 = jnp.zeros((32, LANES), F32)
            for cb in range(blocks):
                cols = pl.ds(cb * LANES, LANES)
                gain = gain_ref[:, cols]
                xhat = (conv[cb, pl.ds(r0, 32), :] - m) * rs
                nrm = xhat * gain + bias_ref[:, cols]
                sig = jax.nn.sigmoid(nrm)
                act[pl.ds(r0, 32), cols] = (nrm * sig).astype(BF16)
                gn = gact[cb, pl.ds(r0, 32), :] * sig * (1.0 + nrm * (1.0 - sig))
                conv[cb, pl.ds(r0, 32), :] = xhat
                gx = gn * gain
                gnorm[cb, pl.ds(r0, 32), :] = gx
                gxx = gx * xhat
                s1 = s1 + gx
                s2 = s2 + gxx
                tacc[cb, taps_n] += jnp.sum((gn * xhat).reshape(4, 8, LANES), axis=0)
                tacc[cb, taps_n + 1] += jnp.sum(gn.reshape(4, 8, LANES), axis=0)
            stage[0, pl.ds(l0, 32), :] = s1
            stage[1, pl.ds(l0, 32), :] = s2

        send_stats(stat2_out, stat2_in, stat2_sem, j)

    for j in order:
        norm_chunk(j)

    per = LANES // share

    @pl.loop(0, model // LANES)
    def _(b):
        part = lax.dot_general(
            grad[:, lanes(b)], act[...], (((0,), (0,)), ((), ())),
            preferred_element_type=F32,
        )
        full[pl.ds(b * per, per)] = part.reshape(per, share, width)

    def pair_copy(i):
        return remote(
            pair_out.at[i], pair_in.at[i], pair_s.at[i], pair_r.at[i], {"sp": partner}
        )

    def ring_copy(i):
        return remote(
            ring_out.at[i], ring_in.at[i], ring_s.at[i], ring_r.at[i],
            {"sp": lax.rem(chip + i, nc) * 2 + par},
        )

    @pl.loop(0, nc)
    def _(i):
        dest = lax.rem(chip + i, nc)
        pair_out[i] = full[dest * 2 + 1 - par].astype(BF16)
        pair_copy(i).start()

    def gconv_chunk(j):
        m1, m2 = recv_stats(stat2_out, stat2_in, stat2_sem, j)
        stage[0] = jnp.broadcast_to(m1, (LANES, LANES)).T
        stage[1] = jnp.broadcast_to(m2, (LANES, LANES)).T

        @pl.loop(0, LANES // 64)
        def _(h):
            l0 = pl.multiple_of(h * 64, 64)
            r0 = pl.multiple_of(j * LANES + l0, 64)
            a = stage[0, pl.ds(l0, 64), :]
            b = stage[1, pl.ds(l0, 64), :]
            rs = rstd_b[pl.ds(r0, 64), :]
            for cb in range(blocks):
                gcpad[cb, pl.ds(r0, 64), :] = rs * (
                    gnorm[cb, pl.ds(r0, 64), :] - a - conv[cb, pl.ds(r0, 64), :] * b
                )

    gconv_chunk(0)
    for cb in range(blocks):
        back_out[cb] = gcpad[cb, pl.ds(0, HALO), :]
    back = remote(back_out, back_in, back_sem.at[0], back_sem.at[1], {"sp": prv})
    back.start()

    @pl.loop(1, nc)
    def _(i):
        dest = lax.rem(chip + i, nc)
        pair_copy(i).wait()
        ring_out[i] = (full[dest * 2 + par] + pair_in[i].astype(F32)).astype(BF16)
        ring_copy(i).start()

    for j in range(1, chunks):
        gconv_chunk(j)

    @pl.loop(0, rows // 64)
    def _(i):
        r0 = pl.multiple_of(i * 64, 64)

        @pl.loop(0, blocks)
        def _(cb):
            gc = gcpad[cb, pl.ds(r0, 64), :]
            for k in range(taps_n):
                prod = gc * gpad[cb, pl.ds(r0 + HALO - taps_n + 1 + k, 64), :]
                tacc[cb, k] += jnp.sum(prod.reshape(8, 8, LANES), axis=0)

    small[...] = jnp.zeros_like(small)
    for cb in range(blocks):
        small[cb, pl.ds(0, taps_n + 2), :] = jnp.sum(tacc[cb], axis=1)
    to_pair = remote(
        small.at[pl.ds((1 - par) * half, half)], small_in, sp_sem.at[0], sp_sem.at[1],
        {"sp": partner},
    )
    to_pair.start()

    def gated_gradient(j):
        @pl.loop(0, LANES // 64)
        def _(h):
            r0 = pl.multiple_of(j * LANES + h * 64, 64)

            @pl.loop(0, blocks)
            def _(cb):
                acc = tap_row(0, cb) * gcpad[cb, pl.ds(r0 + taps_n - 1, 64), :]
                for k in range(1, taps_n):
                    acc = acc + tap_row(k, cb) * gcpad[cb, pl.ds(r0 + taps_n - 1 - k, 64), :]
                v = value[pl.ds(r0, 64), lanes(cb)].astype(F32)
                s = jax.nn.sigmoid(gate[pl.ds(r0, 64), lanes(cb)].astype(F32))
                ds = acc * s
                gv[pl.ds(r0, 64), lanes(cb)] = ds.astype(BF16)
                gg[pl.ds(r0, 64), lanes(cb)] = (ds * v * (1.0 - s)).astype(BF16)

        span = pl.ds(j * LANES, LANES)
        return [
            pltpu.make_async_copy(gv.at[span], gv_hbm.at[span], out_sem.at[0, j]),
            pltpu.make_async_copy(gg.at[span], gg_hbm.at[span], out_sem.at[1, j]),
        ]

    outs = []

    def write(copies):
        for c in copies:
            c.start()
            outs.append(c)

    write(gated_gradient(0))

    to_pair.wait()
    small_all[chip] = small[pl.ds(par * half, half)] + small_in[...]

    def all_copy(i):
        return remote(
            small_all.at[chip], small_all.at[chip], sa_s.at[i], sa_r.at[i],
            {"sp": lax.rem(chip + i, nc) * 2 + par},
        )

    @pl.loop(1, nc)
    def _(i):
        all_copy(i).start()

    for j in range(1, chunks - 1):
        write(gated_gradient(j))

    back.wait()
    last = me == n - 1
    for cb in range(blocks):
        h = back_in[cb]
        gcpad[cb, pl.ds(rows, HALO), :] = jnp.where(last, jnp.zeros_like(h), h)
    write(gated_gradient(chunks - 1))

    pair_copy(0).wait()
    gp[...] = full[me] + pair_in[0].astype(F32)

    @pl.loop(1, nc)
    def _(i):
        ring_copy(i).wait()
        gp[...] += ring_in[i].astype(F32)

    write([pltpu.make_async_copy(gp, gp_hbm, out_sem.at[2, 0])])

    @pl.loop(1, nc)
    def _(i):
        all_copy(i).wait()

    small_tot[...] = small_all[0]

    @pl.loop(1, nc)
    def _(i):
        small_tot[...] += small_all[i]

    fin = remote(small_tot, small_fin, sf_sem.at[0], sf_sem.at[1], {"sp": partner})
    fin.start()
    write([
        pltpu.make_async_copy(
            small_tot, small_hbm.at[pl.ds(par * half, half)], out_sem.at[2, 1]
        )
    ])
    fin.wait()
    write([
        pltpu.make_async_copy(
            small_fin, small_hbm.at[pl.ds((1 - par) * half, half)], out_sem.at[2, 2]
        )
    ])
    for c in outs:
        c.wait()


def on_device(n, tp, value, gate, taps, gain, bias, proj, grad):
    rows, width = value.shape
    model = grad.shape[1]
    taps_n = taps.shape[0]
    blocks = width // LANES
    chunks = rows // LANES
    nc = n // 2
    half = blocks // 2
    share = model // n
    any_spec = pl.BlockSpec(memory_space=pl.ANY)
    vmem = pl.BlockSpec(memory_space=pltpu.VMEM)
    sem = pltpu.SemaphoreType.DMA
    wide = pltpu.VMEM((blocks, rows, LANES), F32)
    padded = pltpu.VMEM((blocks, rows + HALO, LANES), F32)
    gv, gg, small, gp = pl.pallas_call(
        functools.partial(kernel, n, tp, taps_n),
        out_shape=(
            jax.ShapeDtypeStruct((rows, width), BF16),
            jax.ShapeDtypeStruct((rows, width), BF16),
            jax.ShapeDtypeStruct((blocks, SMALL, LANES), F32),
            jax.ShapeDtypeStruct((share, width), F32),
        ),
        in_specs=[any_spec, any_spec, vmem, vmem, vmem, any_spec, any_spec],
        out_specs=(any_spec,) * 4,
        scratch_shapes=[
            pltpu.VMEM((rows, width), BF16),
            pltpu.VMEM((rows, width), BF16),
            pltpu.VMEM((width, model), BF16),
            pltpu.VMEM((rows, model), BF16),
            padded, wide, wide, wide, padded,
            pltpu.VMEM((rows, width), BF16),
            pltpu.VMEM((n, share, width), F32),
            pltpu.VMEM((nc, share, width), BF16),
            pltpu.VMEM((nc, share, width), BF16),
            pltpu.VMEM((nc, share, width), BF16),
            pltpu.VMEM((nc, share, width), BF16),
            pltpu.VMEM((blocks, HALO, LANES), BF16),
            pltpu.VMEM((blocks, HALO, LANES), BF16),
            pltpu.VMEM((blocks, HALO, LANES), F32),
            pltpu.VMEM((blocks, HALO, LANES), F32),
            pltpu.VMEM((2, LANES, LANES), F32),
            pltpu.VMEM((LANES, LANES), F32),
            pltpu.VMEM((rows, LANES), F32),
            pltpu.VMEM((chunks, 8, LANES), F32),
            pltpu.VMEM((chunks, tp - 1, 8, LANES), F32),
            pltpu.VMEM((chunks, 8, LANES), F32),
            pltpu.VMEM((chunks, tp - 1, 8, LANES), F32),
            pltpu.VMEM((blocks, taps_n + 2, 8, LANES), F32),
            pltpu.VMEM((blocks, SMALL, LANES), F32),
            pltpu.VMEM((half, SMALL, LANES), F32),
            pltpu.VMEM((nc, half, SMALL, LANES), F32),
            pltpu.VMEM((half, SMALL, LANES), F32),
            pltpu.VMEM((half, SMALL, LANES), F32),
            pltpu.VMEM((rows, width), BF16),
            pltpu.VMEM((rows, width), BF16),
            pltpu.VMEM((share, width), F32),
            sem((4,)), sem((3, max(chunks, 3))), sem((2,)), sem((2,)),
            sem((2, chunks, tp - 1)), sem((2, chunks, tp - 1)),
            sem((nc,)), sem((nc,)), sem((nc,)), sem((nc,)),
            sem((2,)), sem((nc,)), sem((nc,)), sem((2,)),
        ],
        compiler_params=pltpu.CompilerParams(
            collective_id=0, has_side_effects=True, vmem_limit_bytes=60 * 1024 * 1024
        ),
    )(value, gate, taps, gain.reshape(1, width), bias.reshape(1, width), proj, grad)
    small = small.transpose(1, 0, 2).reshape(SMALL, width)
    return gv, gg, small[:taps_n], small[taps_n], small[taps_n + 1], gp


def solution(mesh):
    n, tp = mesh.shape["sp"], mesh.shape["tp"]
    return jax.shard_map(
        functools.partial(on_device, n, tp),
        mesh=mesh,
        in_specs=(
            P("sp", "tp"),
            P("sp", "tp"),
            P(None, "tp"),
            P("tp"),
            P("tp"),
            P("tp", None),
            P("sp", None),
        ),
        out_specs=(P("sp", "tp"), P("sp", "tp"), P(None, "tp"), P("tp"), P("tp"), P("sp", "tp")),
        check_vma=False,
    )
```

time: 185 us -> 60.6 us (0.33)
  waiting for transfers between devices: 97.3 us -> 0 us
  Pallas kernels: 0 us -> 51.8 us
  blocking collectives: 30.4 us -> 0 us
  other arithmetic: 21.5 us -> 0 us
  between operations: 14.2 us -> 0.66 us
  matrix products: 9.17 us -> 0 us
  starting transfers between devices: 3.9 us -> 0 us
    reduce_scatter x1 -> x0, waiting for transfers between devices: 53.6 us -> none  [on_device(): lax.psum_scatter(lax.dot_general(out_grad, act, (((0,), (0,)), ((), ())),...]
    pallas_call x0 -> x1, Pallas kernels: none -> 51.8 us  [on_device(): pl.pallas_call(functools.partial(kernel, n, tp, taps_n), out_shape=(jax.S...]
    unnamed x3 -> x0, waiting for transfers between devices: 41.8 us -> none
    all_gather x1 -> x0, blocking collectives: 20.3 us -> none  [on_device(): summed = lax.all_gather(share, 'sp', axis=1, tiled=True)]
    reduce_sum x3 -> x0, other arithmetic: 11.6 us -> none  [the longest x2 5.89 us: on_device(): jnp.sum(conv_output_gradient * padded[k:k + rows], axis=0)]
    psum x2 -> x0, blocking collectives: 10.1 us -> none  [the longest x1 5.19 us: on_device(): lax.psum((jnp.sum(conv_output, axis=1), jnp.sum(conv_output * conv_output...]
    convert_element_type x4 -> x0, other arithmetic: 9.87 us -> none  [the longest x1 6.99 us: on_device(): (grad_gated * value * sig_gate * (1.0 - sig_gate)).astype(jnp.bfloat16)]
    dot_general x2 -> x0, matrix products: 9.17 us -> none  [the longest x1 4.61 us: on_device(): lax.dot_general(out_grad, act, (((0,), (0,)), ((), ())), preferred_elemen...]
  transfers between devices with their start and end apart: 4 -> 0, of which waited for: 3 -> 0; matrix products, arithmetic and copies ran while one was open for 9% -> 0% of each run, Pallas kernels for 0% -> 0%
where the time goes in v1:
time: 60.6 us; the launch traced here: 59.8 us
  Pallas kernels  51.8 us (85%)
  local copies, waits for them, and re-layouts  7.34 us (12%)
  between operations  0.66 us (1%)
    pallas_call x1, Pallas kernels, on_device(): pl.pallas_call(functools.partial(kernel, n, tp, taps_n), out_shape=(jax.S...  51.8 us
    unnamed x7, local copies, waits for them, and re-layouts  5.09 us
    slice x3, local copies, waits for them, and re-layouts, on_device(): return (gv, gg, small[:taps_n], small[taps_n], small[taps_n + 1], gp)  2.25 us

profile of v1, /device:TPU:0, one launch (start us, length us, event | category | flops | bytes accessed | tf_op | source)
XLA Modules:
  0.0 59.8 jit_solution(11745743730614355927)
XLA Ops:
  0.6 51.8 %shard_map.118 = (bf16[512,512]{1,0:T(8,128)(2,1)}, bf16[512,512]{1,0:T(8,128)(2,1)}, f32[4,40,128]{2,1,0:T(8,128)}, f32[128,512]{1,0:T(8,128)}) custom-call(bf16[512,512]{1,0:T(8,128)(2,1)} %value_hbm.1, bf16[512,512]{1,0:T(8,128)(2,1)} %gate_hbm.1, f32[31,512]{1,0:T(8,128)} %taps_ref.1, f32[1,512]{1,0:T(1,128)} %bitcast.12, f32[1,512]{1,0:T(1,128)} %bitcast.13, ...), custom_call_target="tpu_custom_call" | custom-call | tf_op jit(solution)/shard_map/pallas_call | solution.py:385
  52.4 0.0 copy-start
  52.4 1.4 %fusion = (f32[1,4,128]{2,0,1:T(1,128)}, f32[1,4,128]{2,0,1:T(1,128)}) fusion(f32[40,4,128]{2,0,1:T(8,128)} %bitcast.10), kind=kLoop, calls=%fused_computation | loop fusion | bytes 8192 | tf_op jit(solution)/shard_map/slice | solution.py:437
  53.8 0.8 %slice.18 = f32[31,4,128]{2,0,1:T(8,128)S(1)} slice(f32[40,4,128]{2,0,1:T(8,128)} %bitcast.11), slice={[0:31], [0:4], [0:128]} | slice | bytes 126976 | tf_op jit(solution)/shard_map/slice | solution.py:437
  54.7 0.6 %copy.14 = f32[4,8,4,128]{3,1,2,0:T(8,128)} copy(f32[4,8,4,128]{3,2,1,0:T(4,128)S(1)} %bitcast.8) | data formatting | bytes 131072
  55.3 1.9 %copy.18 = bf16[512,512]{1,0:T(8,128)(2,1)} copy(bf16[512,512]{1,0:T(8,128)(2,1)} %get-tuple-element.22) | data formatting | bytes 1048576
  57.2 1.9 %copy.19 = bf16[512,512]{1,0:T(8,128)(2,1)} copy(bf16[512,512]{1,0:T(8,128)(2,1)} %get-tuple-element.23) | data formatting | bytes 1048576
  59.1 0.0 copy-done
  59.1 0.7 %copy.20 = f32[128,512]{1,0:T(8,128)} copy(f32[128,512]{1,0:T(8,128)S(1)} %copy-done) | data formatting | bytes 524288
  (2 shorter events, 0.1 us)
Async XLA Ops:
  52.4 6.7 %copy-start = (f32[128,512]{1,0:T(8,128)S(1)}, f32[128,512]{1,0:T(8,128)}, u32[]{:S(2)}) copy-start(f32[128,512]{1,0:T(8,128)} %get-tuple-element.27) | copy-start | bytes 786436

commit v2 on v1

--- a/solution.py
+++ b/solution.py
@@ -15,17 +15,16 @@
 
 
 def kernel(
-    n, tp, taps_n,
+    n, tp, taps_n, ysize,
     value_hbm, gate_hbm, taps_ref, gain_ref, bias_ref, proj_hbm, grad_hbm,
-    gv_hbm, gg_hbm, small_hbm, gp_hbm,
+    gv, gg, gp, taps_out, gain_out, bias_out,
     value, gate, proj, grad, gpad, conv, gact, gnorm, gcpad, act,
-    full, pair_out, pair_in, ring_out, ring_in,
+    grad_t, full, pair_out, pair_in, y_out, y_in, z_out, z_in,
     halo_out, halo_in, back_out, back_in,
     stage, mean_b, rstd_b, stat_out, stat_in, stat2_out, stat2_in,
-    tacc, small, small_in, small_all, small_fin, small_tot,
-    gv, gg, gp,
-    in_sem, out_sem, halo_sem, back_sem, stat_sem, stat2_sem,
-    pair_s, pair_r, ring_s, ring_r, sp_sem, sa_s, sa_r, sf_sem,
+    tacc, small, small_in, small_y, small_z, small_fin, small_tot,
+    in_sem, halo_sem, back_sem, stat_sem, stat2_sem,
+    pair_sem, y_sem, z_sem, sp_sem, sy_sem, sz_sem, sf_sem,
 ):
     rows, width = value.shape
     blocks = width // LANES
@@ -40,6 +39,10 @@
     par = lax.rem(me, 2)
     chip = me // 2
     partner = chip * 2 + 1 - par
+    zsize = nc // ysize
+    cy = lax.rem(chip, ysize)
+    cz = chip // ysize
+    zorder = list(range(zsize // 2, zsize)) + list(range(1, zsize // 2)) + [0]
     nxt = lax.rem(me + 1, n)
     prv = lax.rem(me + n - 1, n)
 
@@ -131,6 +134,12 @@
                 for k in range(1, taps_n):
                     acc = acc + tap_row(k, cb) * gpad[cb, pl.ds(r0 + HALO - taps_n + 1 + k, 64), :]
                 conv[cb, pl.ds(r0, 64), :] = acc
+                step = (j * (LANES // 64) + h) * blocks + cb
+                for e in range(per_step):
+                    tile = step * per_step + e
+                    across = pl.ds(pl.multiple_of(tile % chunks * LANES, LANES), LANES)
+                    down = pl.ds(pl.multiple_of(tile // chunks * LANES, LANES), LANES)
+                    grad_t[down, across] = grad[across, down].T
                 return s + acc, q + acc * acc
 
             zero = jnp.zeros((64, LANES), F32)
@@ -140,6 +149,8 @@
         send_stats(stat_out, stat_in, stat_sem, j)
 
     order = list(range(1, chunks)) + [0]
+    per_step = (model // LANES) * chunks // (chunks * (LANES // 64) * blocks)
+    loads[2].wait()
     for j in order:
         if j == 0:
             halo.wait()
@@ -149,13 +160,14 @@
                 gpad[cb, pl.ds(0, HALO), :] = jnp.where(first, jnp.zeros_like(h), h)
         conv_chunk(j)
 
-    loads[2].wait()
     loads[3].wait()
-    for cb in range(blocks):
-        gact[cb] = lax.dot_general(
-            grad[...], proj[pl.ds(cb * LANES, LANES), :], (((1,), (1,)), ((), ())),
+    for cb in range(0, blocks, 2):
+        both = lax.dot_general(
+            grad[...], proj[pl.ds(cb * LANES, 2 * LANES), :], (((1,), (1,)), ((), ())),
             preferred_element_type=F32,
         )
+        gact[cb] = both[:, :LANES]
+        gact[cb + 1] = both[:, LANES:]
 
     tacc[...] = jnp.zeros_like(tacc)
 
@@ -197,32 +209,58 @@
     for j in order:
         norm_chunk(j)
 
-    per = LANES // share
-
-    @pl.loop(0, model // LANES)
-    def _(b):
+    def owners(k):
+        return lax.rem(cz + zorder[k], zsize) * 2 * ysize
+
+    def pair_copy(k):
+        return remote(
+            pair_out.at[k], pair_in.at[k], pair_sem.at[0, k], pair_sem.at[1, k],
+            {"sp": partner},
+        )
+
+    def y_copy(k, i):
+        return remote(
+            y_out.at[k, i - 1], y_in.at[k, i - 1], y_sem.at[0, k, i - 1],
+            y_sem.at[1, k, i - 1],
+            {"sp": (cz * ysize + lax.rem(cy + i, ysize)) * 2 + par},
+        )
+
+    def z_copy(k):
+        return remote(
+            z_out.at[k], z_in.at[k], z_sem.at[0, k], z_sem.at[1, k],
+            {"sp": (lax.rem(cz + zorder[k], zsize) * ysize + cy) * 2 + par},
+        )
+
+    def pair_stage(k):
+        base = owners(k)
+        span = 2 * ysize * share
         part = lax.dot_general(
-            grad[:, lanes(b)], act[...], (((0,), (0,)), ((), ())),
-            preferred_element_type=F32,
-        )
-        full[pl.ds(b * per, per)] = part.reshape(per, share, width)
-
-    def pair_copy(i):
-        return remote(
-            pair_out.at[i], pair_in.at[i], pair_s.at[i], pair_r.at[i], {"sp": partner}
-        )
-
-    def ring_copy(i):
-        return remote(
-            ring_out.at[i], ring_in.at[i], ring_s.at[i], ring_r.at[i],
-            {"sp": lax.rem(chip + i, nc) * 2 + par},
-        )
-
-    @pl.loop(0, nc)
-    def _(i):
-        dest = lax.rem(chip + i, nc)
-        pair_out[i] = full[dest * 2 + 1 - par].astype(BF16)
-        pair_copy(i).start()
+            grad_t[pl.ds(pl.multiple_of(base * share, LANES), span), :], act[...],
+            (((1,), (0,)), ((), ())), preferred_element_type=F32,
+        )
+        full[pl.ds(base, 2 * ysize)] = part.reshape(2 * ysize, share, width)
+        for y in range(ysize):
+            pair_out[k, y] = full[base + 2 * y + 1 - par].astype(BF16)
+        pair_copy(k).start()
+
+    def y_stage(k):
+        base = owners(k)
+        pair_copy(k).wait()
+        for i in range(1, ysize):
+            y = lax.rem(cy + i, ysize)
+            y_out[k, i - 1] = (full[base + 2 * y + par] + pair_in[k, y].astype(F32)).astype(BF16)
+            y_copy(k, i).start()
+
+    def z_stage(k):
+        acc = full[owners(k) + 2 * cy + par] + pair_in[k, cy].astype(F32)
+        for i in range(1, ysize):
+            y_copy(k, i).wait()
+            acc = acc + y_in[k, i - 1].astype(F32)
+        if zorder[k]:
+            z_out[k] = acc.astype(BF16)
+            z_copy(k).start()
+        else:
+            gp[...] = acc
 
     def gconv_chunk(j):
         m1, m2 = recv_stats(stat2_out, stat2_in, stat2_sem, j)
@@ -241,32 +279,39 @@
                     gnorm[cb, pl.ds(r0, 64), :] - a - conv[cb, pl.ds(r0, 64), :] * b
                 )
 
-    gconv_chunk(0)
-    for cb in range(blocks):
-        back_out[cb] = gcpad[cb, pl.ds(0, HALO), :]
+    def send_back():
+        gconv_chunk(0)
+        for cb in range(blocks):
+            back_out[cb] = gcpad[cb, pl.ds(0, HALO), :]
+        back.start()
+
     back = remote(back_out, back_in, back_sem.at[0], back_sem.at[1], {"sp": prv})
-    back.start()
-
-    @pl.loop(1, nc)
-    def _(i):
-        dest = lax.rem(chip + i, nc)
-        pair_copy(i).wait()
-        ring_out[i] = (full[dest * 2 + par] + pair_in[i].astype(F32)).astype(BF16)
-        ring_copy(i).start()
-
+
+    def taps_rows(first, count):
+        @pl.loop(first, first + count)
+        def _(i):
+            r0 = pl.multiple_of(i * 64, 64)
+
+            @pl.loop(0, blocks)
+            def _(cb):
+                gc = gcpad[cb, pl.ds(r0, 64), :]
+                for k in range(taps_n):
+                    prod = gc * gpad[cb, pl.ds(r0 + HALO - taps_n + 1 + k, 64), :]
+                    tacc[cb, k] += jnp.sum(prod.reshape(8, 8, LANES), axis=0)
+
+    for k in range(zsize):
+        pair_stage(k)
+        if k == 1:
+            send_back()
+        if k >= 1:
+            y_stage(k - 1)
     for j in range(1, chunks):
         gconv_chunk(j)
 
-    @pl.loop(0, rows // 64)
-    def _(i):
-        r0 = pl.multiple_of(i * 64, 64)
-
-        @pl.loop(0, blocks)
-        def _(cb):
-            gc = gcpad[cb, pl.ds(r0, 64), :]
-            for k in range(taps_n):
-                prod = gc * gpad[cb, pl.ds(r0 + HALO - taps_n + 1 + k, 64), :]
-                tacc[cb, k] += jnp.sum(prod.reshape(8, 8, LANES), axis=0)
+    steps = rows // 64
+    taps_rows(0, steps // 2)
+    z_stage(0)
+    taps_rows(steps // 2, steps - steps // 2)
 
     small[...] = jnp.zeros_like(small)
     for cb in range(blocks):
@@ -293,79 +338,71 @@
                 gv[pl.ds(r0, 64), lanes(cb)] = ds.astype(BF16)
                 gg[pl.ds(r0, 64), lanes(cb)] = (ds * v * (1.0 - s)).astype(BF16)
 
-        span = pl.ds(j * LANES, LANES)
-        return [
-            pltpu.make_async_copy(gv.at[span], gv_hbm.at[span], out_sem.at[0, j]),
-            pltpu.make_async_copy(gg.at[span], gg_hbm.at[span], out_sem.at[1, j]),
-        ]
-
-    outs = []
-
-    def write(copies):
-        for c in copies:
-            c.start()
-            outs.append(c)
-
-    write(gated_gradient(0))
-
+    z_stage(1)
     to_pair.wait()
-    small_all[chip] = small[pl.ds(par * half, half)] + small_in[...]
-
-    def all_copy(i):
-        return remote(
-            small_all.at[chip], small_all.at[chip], sa_s.at[i], sa_r.at[i],
-            {"sp": lax.rem(chip + i, nc) * 2 + par},
-        )
-
-    @pl.loop(1, nc)
-    def _(i):
-        all_copy(i).start()
-
-    for j in range(1, chunks - 1):
-        write(gated_gradient(j))
+    small_y[cy] = small[pl.ds(par * half, half)] + small_in[...]
+
+    def small_y_copy(i):
+        return remote(
+            small_y.at[cy], small_y.at[cy], sy_sem.at[0, i - 1], sy_sem.at[1, i - 1],
+            {"sp": (cz * ysize + lax.rem(cy + i, ysize)) * 2 + par},
+        )
+
+    def small_z_copy(i):
+        return remote(
+            small_z.at[cz], small_z.at[cz], sz_sem.at[0, i - 1], sz_sem.at[1, i - 1],
+            {"sp": (lax.rem(cz + i, zsize) * ysize + cy) * 2 + par},
+        )
+
+    for i in range(1, ysize):
+        small_y_copy(i).start()
+    y_stage(zsize - 1)
+
+    gated_gradient(0)
+    for k in range(2, zsize - 1):
+        z_stage(k)
+    gated_gradient(1)
+
+    for i in range(1, ysize):
+        small_y_copy(i).wait()
+    total = small_y[0]
+    for i in range(1, ysize):
+        total = total + small_y[i]
+    small_z[cz] = total
+    for i in range(1, zsize):
+        small_z_copy(i).start()
+
+    for j in range(2, chunks - 1):
+        gated_gradient(j)
 
     back.wait()
     last = me == n - 1
     for cb in range(blocks):
         h = back_in[cb]
         gcpad[cb, pl.ds(rows, HALO), :] = jnp.where(last, jnp.zeros_like(h), h)
-    write(gated_gradient(chunks - 1))
-
-    pair_copy(0).wait()
-    gp[...] = full[me] + pair_in[0].astype(F32)
-
-    @pl.loop(1, nc)
-    def _(i):
-        ring_copy(i).wait()
-        gp[...] += ring_in[i].astype(F32)
-
-    write([pltpu.make_async_copy(gp, gp_hbm, out_sem.at[2, 0])])
-
-    @pl.loop(1, nc)
-    def _(i):
-        all_copy(i).wait()
-
-    small_tot[...] = small_all[0]
-
-    @pl.loop(1, nc)
-    def _(i):
-        small_tot[...] += small_all[i]
-
+    gated_gradient(chunks - 1)
+
+    z_stage(zsize - 1)
+    for i in range(1, zsize):
+        small_z_copy(i).wait()
+    total = small_z[0]
+    for i in range(1, zsize):
+        total = total + small_z[i]
+    small_tot[...] = total
     fin = remote(small_tot, small_fin, sf_sem.at[0], sf_sem.at[1], {"sp": partner})
     fin.start()
-    write([
-        pltpu.make_async_copy(
-            small_tot, small_hbm.at[pl.ds(par * half, half)], out_sem.at[2, 1]
-        )
-    ])
+
+    for k in range(zsize - 1):
+        z_copy(k).wait()
+        gp[...] += z_in[k].astype(F32)
+
     fin.wait()
-    write([
-        pltpu.make_async_copy(
-            small_fin, small_hbm.at[pl.ds((1 - par) * half, half)], out_sem.at[2, 2]
-        )
-    ])
-    for c in outs:
-        c.wait()
+    for cb in range(half):
+        for source, where in ((small_tot, par), (small_fin, 1 - par)):
+            cols = lanes(where * half + cb)
+            taps_out[:, cols] = source[cb, pl.ds(0, taps_n), :]
+            gain_out[:, cols] = source[cb, pl.ds(taps_n, 1), :]
+            bias_out[:, cols] = source[cb, pl.ds(taps_n + 1, 1), :]
 
 
 def on_device(n, tp, value, gate, taps, gain, bias, proj, grad):
@@ -377,21 +414,27 @@
     nc = n // 2
     half = blocks // 2
     share = model // n
-    any_spec = pl.BlockSpec(memory_space=pl.ANY)
+    ysize = 1
+    while 2 * (2 * ysize) ** 2 <= nc:
+        ysize *= 2
+    zsize = nc // ysize
+    hbm = pl.BlockSpec(memory_space=pltpu.HBM)
     vmem = pl.BlockSpec(memory_space=pltpu.VMEM)
     sem = pltpu.SemaphoreType.DMA
     wide = pltpu.VMEM((blocks, rows, LANES), F32)
     padded = pltpu.VMEM((blocks, rows + HALO, LANES), F32)
-    gv, gg, small, gp = pl.pallas_call(
-        functools.partial(kernel, n, tp, taps_n),
+    gv, gg, gp, dtaps, dgain, dbias = pl.pallas_call(
+        functools.partial(kernel, n, tp, taps_n, ysize),
         out_shape=(
             jax.ShapeDtypeStruct((rows, width), BF16),
             jax.ShapeDtypeStruct((rows, width), BF16),
-            jax.ShapeDtypeStruct((blocks, SMALL, LANES), F32),
             jax.ShapeDtypeStruct((share, width), F32),
+            jax.ShapeDtypeStruct((taps_n, width), F32),
+            jax.ShapeDtypeStruct((1, width), F32),
+            jax.ShapeDtypeStruct((1, width), F32),
         ),
-        in_specs=[any_spec, any_spec, vmem, vmem, vmem, any_spec, any_spec],
-        out_specs=(any_spec,) * 4,
+        in_specs=[hbm, hbm, vmem, vmem, vmem, hbm, hbm],
+        out_specs=(vmem,) * 6,
         scratch_shapes=[
             pltpu.VMEM((rows, width), BF16),
             pltpu.VMEM((rows, width), BF16),
@@ -399,11 +442,14 @@
             pltpu.VMEM((rows, model), BF16),
             padded, wide, wide, wide, padded,
             pltpu.VMEM((rows, width), BF16),
+            pltpu.VMEM((model, rows), BF16),
             pltpu.VMEM((n, share, width), F32),
-            pltpu.VMEM((nc, share, width), BF16),
-            pltpu.VMEM((nc, share, width), BF16),
-            pltpu.VMEM((nc, share, width), BF16),
-            pltpu.VMEM((nc, share, width), BF16),
+            pltpu.VMEM((zsize, ysize, share, width), BF16),
+            pltpu.VMEM((zsize, ysize, share, width), BF16),
+            pltpu.VMEM((zsize, ysize - 1, share, width), BF16),
+            pltpu.VMEM((zsize, ysize - 1, share, width), BF16),
+            pltpu.VMEM((zsize - 1, share, width), BF16),
+            pltpu.VMEM((zsize - 1, share, width), BF16),
             pltpu.VMEM((blocks, HALO, LANES), BF16),
             pltpu.VMEM((blocks, HALO, LANES), BF16),
             pltpu.VMEM((blocks, HALO, LANES), F32),
@@ -418,23 +464,20 @@
             pltpu.VMEM((blocks, taps_n + 2, 8, LANES), F32),
             pltpu.VMEM((blocks, SMALL, LANES), F32),
             pltpu.VMEM((half, SMALL, LANES), F32),
-            pltpu.VMEM((nc, half, SMALL, LANES), F32),
+            pltpu.VMEM((ysize, half, SMALL, LANES), F32),
+            pltpu.VMEM((zsize, half, SMALL, LANES), F32),
             pltpu.VMEM((half, SMALL, LANES), F32),
             pltpu.VMEM((half, SMALL, LANES), F32),
-            pltpu.VMEM((rows, width), BF16),
-            pltpu.VMEM((rows, width), BF16),
-            pltpu.VMEM((share, width), F32),
-            sem((4,)), sem((3, max(chunks, 3))), sem((2,)), sem((2,)),
+            sem((4,)), sem((2,)), sem((2,)),
             sem((2, chunks, tp - 1)), sem((2, chunks, tp - 1)),
-            sem((nc,)), sem((nc,)), sem((nc,)), sem((nc,)),
-            sem((2,)), sem((nc,)), sem((nc,)), sem((2,)),
+            sem((2, zsize)), sem((2, zsize, ysize - 1)), sem((2, zsize - 1)),
+            sem((2,)), sem((2, ysize - 1)), sem((2, zsize - 1)), sem((2,)),
         ],
         compiler_params=pltpu.CompilerParams(
-            collective_id=0, has_side_effects=True, vmem_limit_bytes=60 * 1024 * 1024
+            collective_id=0, has_side_effects=True, vmem_limit_bytes=36 * 1024 * 1024
         ),
     )(value, gate, taps, gain.reshape(1, width), bias.reshape(1, width), proj, grad)
-    small = small.transpose(1, 0, 2).reshape(SMALL, width)
-    return gv, gg, small[:taps_n], small[taps_n], small[taps_n + 1], gp
+    return gv, gg, dtaps, dgain.reshape(width), dbias.reshape(width), gp
 
 
 def solution(mesh):

time: 60.6 us -> 51.9 us (0.86)
  Pallas kernels: 51.8 us -> 39.3 us
  local copies, waits for them, and re-layouts: 7.34 us -> 11.5 us
    pallas_call x1, Pallas kernels: 51.8 us -> 39.3 us  [on_device(): pl.pallas_call(functools.partial(kernel, n, tp, taps_n, ysize), out_shape...]
    unnamed x7 -> x20, local copies, waits for them, and re-layouts: 5.09 us -> 11.5 us
    slice x3 -> x0, local copies, waits for them, and re-layouts: 2.25 us -> none  [on_device(): return (gv, gg, small[:taps_n], small[taps_n], small[taps_n + 1], gp)]
where the time goes in v2:
time: 51.9 us; the launch traced here: 51.5 us
  Pallas kernels  39.3 us (76%)
  local copies, waits for them, and re-layouts  11.5 us (22%)
  between operations  0.66 us (1%)
    pallas_call x1, Pallas kernels, on_device(): pl.pallas_call(functools.partial(kernel, n, tp, taps_n, ysize), out_shape...  39.3 us
    unnamed x20, local copies, waits for them, and re-layouts  11.5 us

profile of v2, /device:TPU:0, one launch (start us, length us, event | category | flops | bytes accessed | tf_op | source)
XLA Modules:
  0.0 51.5 jit_solution(1907411770357687167)
XLA Ops:
  0.6 0.0 copy-start
  0.6 1.6 %copy-done = bf16[512,2048]{1,0:T(8,128)(2,1)S(1)} copy-done((bf16[512,2048]{1,0:T(8,128)(2,1)S(1)}, bf16[512,2048]{1,0:T(8,128)(2,1)}, u32[]{:S(2)}) %copy-start) | copy-done | bytes 2097176
  2.2 0.0 copy-start.1
  2.2 1.6 %copy-done.1 = bf16[512,2048]{1,0:T(8,128)(2,1)S(1)} copy-done((bf16[512,2048]{1,0:T(8,128)(2,1)S(1)}, bf16[512,2048]{1,0:T(8,128)(2,1)}, u32[]{:S(2)}) %copy-start.1) | copy-done | bytes 2097176
  3.8 0.0 copy-start.2
  3.8 1.0 %copy-done.2 = bf16[512,512]{1,0:T(8,128)(2,1)S(1)} copy-done((bf16[512,512]{1,0:T(8,128)(2,1)S(1)}, bf16[512,512]{1,0:T(8,128)(2,1)}, u32[]{:S(2)}) %copy-start.2) | copy-done | bytes 524312
  4.9 0.0 copy-start.3
  4.9 1.0 %copy-done.3 = bf16[512,512]{1,0:T(8,128)(2,1)S(1)} copy-done((bf16[512,512]{1,0:T(8,128)(2,1)S(1)}, bf16[512,512]{1,0:T(8,128)(2,1)}, u32[]{:S(2)}) %copy-start.3) | copy-done | bytes 524312
  5.9 0.0 copy-start.4
  5.9 0.8 %copy-done.4 = f32[31,512]{1,0:T(8,128)S(1)} copy-done((f32[31,512]{1,0:T(8,128)S(1)}, f32[31,512]{1,0:T(8,128)}, u32[]{:S(2)}) %copy-start.4) | copy-done | bytes 63512
  6.7 0.0 copy-start.5
  6.7 0.7 %copy-done.5 = f32[512]{0:T(512)S(1)} copy-done((f32[512]{0:T(512)S(1)}, f32[512]{0:T(512)}, u32[]{:S(2)}) %copy-start.5) | copy-done | bytes 2072
  7.4 0.0 copy-start.6
  7.4 0.7 %copy-done.6 = f32[512]{0:T(512)S(1)} copy-done((f32[512]{0:T(512)S(1)}, f32[512]{0:T(512)}, u32[]{:S(2)}) %copy-start.6) | copy-done | bytes 2072
  8.1 39.3 %shard_map.118 = (bf16[512,512]{1,0:T(8,128)(2,1)S(1)}, bf16[512,512]{1,0:T(8,128)(2,1)S(1)}, f32[128,512]{1,0:T(8,128)S(1)}, f32[31,512]{1,0:T(8,128)S(1)}, f32[1,512]{1,0:T(1,128)S(1)}, /*index=5*/f32[1,512]{1,0:T(1,128)S(1)}) custom-call(bf16[512,512]{1,0:T(8,128)(2,1)S(1)} %copy-done.2, bf16[512,512]{1,0:T(8,128)(2,1)S(1)} %copy-done.3, ...), custom_call_target="tpu_custom_call" | custom-call | tf_op jit(solution)/shard_map/pallas_call | solution.py:426
  47.4 0.8 %copy.19 = bf16[512,512]{1,0:T(8,128)(2,1)} copy(bf16[512,512]{1,0:T(8,128)(2,1)S(1)} %get-tuple-element.24) | data formatting | bytes 1048576
  48.2 0.8 %copy.20 = bf16[512,512]{1,0:T(8,128)(2,1)} copy(bf16[512,512]{1,0:T(8,128)(2,1)S(1)} %get-tuple-element.25) | data formatting | bytes 1048576
  49.0 0.6 %copy.21 = f32[31,512]{1,0:T(8,128)} copy(f32[31,512]{1,0:T(8,128)S(1)} %get-tuple-element.26) | data formatting | bytes 126976
  49.7 0.6 %copy.22 = f32[512]{0:T(512)} copy(f32[512]{0:T(512)S(1)} %bitcast.7) | data formatting | bytes 4096
  50.2 0.6 %copy.23 = f32[512]{0:T(512)} copy(f32[512]{0:T(512)S(1)} %bitcast.6) | data formatting | bytes 4096
  50.8 0.7 %copy.24 = f32[128,512]{1,0:T(8,128)} copy(f32[128,512]{1,0:T(8,128)S(1)} %get-tuple-element.29) | data formatting | bytes 524288
Async XLA Ops:
  0.6 1.6 %copy-start = (bf16[512,2048]{1,0:T(8,128)(2,1)S(1)}, bf16[512,2048]{1,0:T(8,128)(2,1)}, u32[]{:S(2)}) copy-start(bf16[512,2048]{1,0:T(8,128)(2,1)} %proj_hbm.1) | copy-start | bytes 6291460
  2.2 1.6 %copy-start.1 = (bf16[512,2048]{1,0:T(8,128)(2,1)S(1)}, bf16[512,2048]{1,0:T(8,128)(2,1)}, u32[]{:S(2)}) copy-start(bf16[512,2048]{1,0:T(8,128)(2,1)} %grad_hbm.1) | copy-start | bytes 6291460
  3.8 1.0 %copy-start.2 = (bf16[512,512]{1,0:T(8,128)(2,1)S(1)}, bf16[512,512]{1,0:T(8,128)(2,1)}, u32[]{:S(2)}) copy-start(bf16[512,512]{1,0:T(8,128)(2,1)} %value_hbm.1) | copy-start | bytes 1572868
  4.9 1.0 %copy-start.3 = (bf16[512,512]{1,0:T(8,128)(2,1)S(1)}, bf16[512,512]{1,0:T(8,128)(2,1)}, u32[]{:S(2)}) copy-start(bf16[512,512]{1,0:T(8,128)(2,1)} %gate_hbm.1) | copy-start | bytes 1572868
  5.9 0.8 %copy-start.4 = (f32[31,512]{1,0:T(8,128)S(1)}, f32[31,512]{1,0:T(8,128)}, u32[]{:S(2)}) copy-start(f32[31,512]{1,0:T(8,128)} %taps_ref.1) | copy-start | bytes 190468
  6.7 0.7 %copy-start.5 = (f32[512]{0:T(512)S(1)}, f32[512]{0:T(512)}, u32[]{:S(2)}) copy-start(f32[512]{0:T(512)} %param.10) | copy-start | bytes 6148
  7.4 0.7 %copy-start.6 = (f32[512]{0:T(512)S(1)}, f32[512]{0:T(512)}, u32[]{:S(2)}) copy-start(f32[512]{0:T(512)} %param.11) | copy-start | bytes 6148

commit v3 on v2

--- a/solution.py
+++ b/solution.py
@@ -16,13 +16,13 @@
 
 def kernel(
     n, tp, taps_n, ysize,
-    value_hbm, gate_hbm, taps_ref, gain_ref, bias_ref, proj_hbm, grad_hbm,
+    value_hbm, gate_hbm, taps_hbm, gain_hbm, bias_hbm, proj_hbm, grad_hbm,
     gv, gg, gp, taps_out, gain_out, bias_out,
-    value, gate, proj, grad, gpad, conv, gact, gnorm, gcpad, act,
+    value, gate, taps_ref, gain_ref, bias_ref, proj, grad, gpad, conv, gact, gnorm, gcpad, act,
     grad_t, full, pair_out, pair_in, y_out, y_in, z_out, z_in,
     halo_out, halo_in, back_out, back_in,
     stage, mean_b, rstd_b, stat_out, stat_in, stat2_out, stat2_in,
-    tacc, small, small_in, small_y, small_z, small_fin, small_tot,
+    tacc, small, small_in, small_y, small_z, small_zin, small_fin, small_tot,
     in_sem, halo_sem, back_sem, stat_sem, stat2_sem,
     pair_sem, y_sem, z_sem, sp_sem, sy_sem, sz_sem, sf_sem,
 ):
@@ -49,11 +49,14 @@
     loads = [
         pltpu.make_async_copy(s, d, in_sem.at[i])
         for i, (s, d) in enumerate(
-            ((value_hbm, value), (gate_hbm, gate), (grad_hbm, grad), (proj_hbm, proj))
+            (
+                (value_hbm, value), (gate_hbm, gate), (grad_hbm, grad), (proj_hbm, proj),
+                (taps_hbm, taps_ref), (gain_hbm, gain_ref), (bias_hbm, bias_ref),
+            )
         )
     ]
-    for c in loads:
-        c.start()
+    for i in (0, 1, 4, 2, 3, 5, 6):
+        loads[i].start()
 
     barrier = pltpu.get_barrier_semaphore()
 
@@ -111,9 +114,7 @@
     for cb in range(blocks):
         g = gated_rows(rows - HALO, cb, HALO)
         halo_out[cb] = g
-    pl.semaphore_wait(barrier, n - 1 + tp - 1)
     halo = remote(halo_out, halo_in, halo_sem.at[0], halo_sem.at[1], {"sp": nxt})
-    halo.start()
 
     @pl.loop(0, rows // 64)
     def _(i):
@@ -130,26 +131,33 @@
 
             def body(cb, carry):
                 s, q = carry
+                step = (j * (LANES // 64) + h) * blocks + cb
+                tiles = []
+                for e in range(per_step):
+                    tile = step * per_step + e
+                    across = pl.ds(pl.multiple_of(tile % chunks * LANES, LANES), LANES)
+                    down = pl.ds(pl.multiple_of(tile // chunks * LANES, LANES), LANES)
+                    tiles.append((down, across, grad[across, down].T))
                 acc = tap_row(0, cb) * gpad[cb, pl.ds(r0 + 2, 64), :]
                 for k in range(1, taps_n):
                     acc = acc + tap_row(k, cb) * gpad[cb, pl.ds(r0 + HALO - taps_n + 1 + k, 64), :]
                 conv[cb, pl.ds(r0, 64), :] = acc
-                step = (j * (LANES // 64) + h) * blocks + cb
-                for e in range(per_step):
-                    tile = step * per_step + e
-                    across = pl.ds(pl.multiple_of(tile % chunks * LANES, LANES), LANES)
-                    down = pl.ds(pl.multiple_of(tile // chunks * LANES, LANES), LANES)
-                    grad_t[down, across] = grad[across, down].T
+                for down, across, tile in tiles:
+                    grad_t[down, across] = tile
                 return s + acc, q + acc * acc
 
             zero = jnp.zeros((64, LANES), F32)
             s, q = lax.fori_loop(0, blocks, body, (zero, zero))
             stage[0, pl.ds(h * 64, 64), :] = s
             stage[1, pl.ds(h * 64, 64), :] = q
+        if j == 1:
+            pl.semaphore_wait(barrier, n - 1 + tp - 1)
+            halo.start()
         send_stats(stat_out, stat_in, stat_sem, j)
 
     order = list(range(1, chunks)) + [0]
     per_step = (model // LANES) * chunks // (chunks * (LANES // 64) * blocks)
+    loads[4].wait()
     loads[2].wait()
     for j in order:
         if j == 0:
@@ -161,6 +169,8 @@
         conv_chunk(j)
 
     loads[3].wait()
+    loads[5].wait()
+    loads[6].wait()
     for cb in range(0, blocks, 2):
         both = lax.dot_general(
             grad[...], proj[pl.ds(cb * LANES, 2 * LANES), :], (((1,), (1,)), ((), ())),
@@ -303,10 +313,11 @@
         pair_stage(k)
         if k == 1:
             send_back()
-        if k >= 1:
-            y_stage(k - 1)
+        if k >= 2:
+            y_stage(k - 2)
     for j in range(1, chunks):
         gconv_chunk(j)
+    y_stage(zsize - 2)
 
     steps = rows // 64
     taps_rows(0, steps // 2)
@@ -349,9 +360,11 @@
         )
 
     def small_z_copy(i):
+        d = 2**i
+        other = cz + d - 2 * d * lax.rem(cz // d, 2)
         return remote(
-            small_z.at[cz], small_z.at[cz], sz_sem.at[0, i - 1], sz_sem.at[1, i - 1],
-            {"sp": (lax.rem(cz + i, zsize) * ysize + cy) * 2 + par},
+            small_z.at[i], small_zin.at[i], sz_sem.at[0, i], sz_sem.at[1, i],
+            {"sp": (other * ysize + cy) * 2 + par},
         )
 
     for i in range(1, ysize):
@@ -368,12 +381,20 @@
     total = small_y[0]
     for i in range(1, ysize):
         total = total + small_y[i]
-    small_z[cz] = total
-    for i in range(1, zsize):
-        small_z_copy(i).start()
+    rounds = zsize.bit_length() - 1
+    small_z[0] = total
+    small_z_copy(0).start()
 
     for j in range(2, chunks - 1):
         gated_gradient(j)
+
+    def next_round(i):
+        small_z_copy(i).wait()
+        both = small_z[i] + small_zin[i]
+        if i + 1 < rounds:
+            small_z[i + 1] = both
+            small_z_copy(i + 1).start()
+        return both
 
     back.wait()
     last = me == n - 1
@@ -383,11 +404,8 @@
     gated_gradient(chunks - 1)
 
     z_stage(zsize - 1)
-    for i in range(1, zsize):
-        small_z_copy(i).wait()
-    total = small_z[0]
-    for i in range(1, zsize):
-        total = total + small_z[i]
+    for i in range(rounds):
+        total = next_round(i)
     small_tot[...] = total
     fin = remote(small_tot, small_fin, sf_sem.at[0], sf_sem.at[1], {"sp": partner})
     fin.start()
@@ -403,6 +421,15 @@
             taps_out[:, cols] = source[cb, pl.ds(0, taps_n), :]
             gain_out[:, cols] = source[cb, pl.ds(taps_n, 1), :]
             bias_out[:, cols] = source[cb, pl.ds(taps_n + 1, 1), :]
+
+
+def write_out(*refs):
+    sems = refs[12]
+    copies = [pltpu.make_async_copy(refs[i], refs[6 + i], sems.at[i]) for i in range(6)]
+    for c in copies:
+        c.start()
+    for c in copies:
+        c.wait()
 
 
 def on_device(n, tp, value, gate, taps, gain, bias, proj, grad):
@@ -433,11 +460,14 @@
             jax.ShapeDtypeStruct((1, width), F32),
             jax.ShapeDtypeStruct((1, width), F32),
         ),
-        in_specs=[hbm, hbm, vmem, vmem, vmem, hbm, hbm],
+        in_specs=[hbm] * 7,
         out_specs=(vmem,) * 6,
         scratch_shapes=[
             pltpu.VMEM((rows, width), BF16),
             pltpu.VMEM((rows, width), BF16),
+            pltpu.VMEM((taps_n, width), F32),
+            pltpu.VMEM((1, width), F32),
+            pltpu.VMEM((1, width), F32),
             pltpu.VMEM((width, model), BF16),
             pltpu.VMEM((rows, model), BF16),
             padded, wide, wide, wide, padded,
@@ -465,18 +495,35 @@
             pltpu.VMEM((blocks, SMALL, LANES), F32),
             pltpu.VMEM((half, SMALL, LANES), F32),
             pltpu.VMEM((ysize, half, SMALL, LANES), F32),
-            pltpu.VMEM((zsize, half, SMALL, LANES), F32),
+            pltpu.VMEM((zsize.bit_length() - 1, half, SMALL, LANES), F32),
+            pltpu.VMEM((zsize.bit_length() - 1, half, SMALL, LANES), F32),
             pltpu.VMEM((half, SMALL, LANES), F32),
             pltpu.VMEM((half, SMALL, LANES), F32),
-            sem((4,)), sem((2,)), sem((2,)),
+            sem((7,)), sem((2,)), sem((2,)),
             sem((2, chunks, tp - 1)), sem((2, chunks, tp - 1)),
             sem((2, zsize)), sem((2, zsize, ysize - 1)), sem((2, zsize - 1)),
-            sem((2,)), sem((2, ysize - 1)), sem((2, zsize - 1)), sem((2,)),
+            sem((2,)), sem((2, ysize - 1)), sem((2, zsize.bit_length() - 1)), sem((2,)),
         ],
         compiler_params=pltpu.CompilerParams(
             collective_id=0, has_side_effects=True, vmem_limit_bytes=36 * 1024 * 1024
         ),
-    )(value, gate, taps, gain.reshape(1, width), bias.reshape(1, width), proj, grad)
+    )(
+        *(
+            pltpu.with_memory_space_constraint(x, pltpu.HBM)
+            for x in (
+                value, gate, taps, gain.reshape(1, width), bias.reshape(1, width), proj, grad
+            )
+        )
+    )
+    results = (gv, gg, gp, dtaps, dgain, dbias)
+    gv, gg, gp, dtaps, dgain, dbias = pl.pallas_call(
+        write_out,
+        out_shape=[jax.ShapeDtypeStruct(r.shape, r.dtype) for r in results],
+        in_specs=[pl.BlockSpec(memory_space=pl.ANY)] * 6,
+        out_specs=[hbm] * 6,
+        scratch_shapes=[sem((6,))],
+        compiler_params=pltpu.CompilerParams(vmem_limit_bytes=1024 * 1024),
+    )(*results)
     return gv, gg, dtaps, dgain.reshape(width), dbias.reshape(width), gp
 
 

time: 51.9 us -> 41.1 us (0.79)
  local copies, waits for them, and re-layouts: 11.5 us -> 0 us
  Pallas kernels: 39.3 us -> 40.3 us
    unnamed x20 -> x0, local copies, waits for them, and re-layouts: 11.5 us -> none
    pallas_call x0 -> x1, Pallas kernels: none -> 1.12 us  [on_device(): pl.pallas_call(write_out, out_shape=[jax.ShapeDtypeStruct(r.shape, r.dtyp...]
where the time goes in v3:
time: 41.1 us; the launch traced here: 40.9 us
  Pallas kernels  40.3 us (98%)
  between operations  0.64 us (2%)
    pallas_call x1, Pallas kernels, on_device(): pl.pallas_call(functools.partial(kernel, n, tp, taps_n, ysize), out_shape...  39.1 us
    pallas_call x1, Pallas kernels, on_device(): pl.pallas_call(write_out, out_shape=[jax.ShapeDtypeStruct(r.shape, r.dtyp...  1.12 us

profile of v3, /device:TPU:0, one launch (start us, length us, event | category | flops | bytes accessed | tf_op | source)
XLA Modules:
  0.0 40.9 jit_solution(10119952917739435417)
XLA Ops:
  0.6 39.1 %shard_map.118 = (bf16[512,512]{1,0:T(8,128)(2,1)S(1)}, bf16[512,512]{1,0:T(8,128)(2,1)S(1)}, f32[128,512]{1,0:T(8,128)S(1)}, f32[31,512]{1,0:T(8,128)S(1)}, f32[1,512]{1,0:T(1,128)S(1)}, /*index=5*/f32[1,512]{1,0:T(1,128)S(1)}) custom-call(bf16[512,512]{1,0:T(8,128)(2,1)} %value_hbm.1, bf16[512,512]{1,0:T(8,128)(2,1)} %gate_hbm.1, f32[31,512]{1,0:T(8,128)} %taps_hbm.1, ...), custom_call_target="tpu_custom_call" | custom-call | tf_op jit(solution)/shard_map/pallas_call | solution.py:453
  39.8 1.1 %shard_map.119 = (bf16[512,512]{1,0:T(8,128)(2,1)}, bf16[512,512]{1,0:T(8,128)(2,1)}, f32[128,512]{1,0:T(8,128)}, f32[31,512]{1,0:T(8,128)}, f32[1,512]{1,0:T(1,128)}, /*index=5*/f32[1,512]{1,0:T(1,128)}) custom-call(bf16[512,512]{1,0:T(8,128)(2,1)S(1)} %get-tuple-element.18.refs_0_, bf16[512,512]{1,0:T(8,128)(2,1)S(1)} %get-tuple-element.19.refs_1_, ...), custom_call_target="tpu_custom_call" | custom-call | tf_op jit(solution)/shard_map/pallas_call | solution.py:519

commit v4 on v3

--- a/solution.py
+++ b/solution.py
@@ -320,9 +320,7 @@
     y_stage(zsize - 2)
 
     steps = rows // 64
-    taps_rows(0, steps // 2)
-    z_stage(0)
-    taps_rows(steps // 2, steps - steps // 2)
+    taps_rows(0, steps)
 
     small[...] = jnp.zeros_like(small)
     for cb in range(blocks):
@@ -349,6 +347,8 @@
                 gv[pl.ds(r0, 64), lanes(cb)] = ds.astype(BF16)
                 gg[pl.ds(r0, 64), lanes(cb)] = (ds * v * (1.0 - s)).astype(BF16)
 
+    z_stage(0)
+    gated_gradient(0)
     z_stage(1)
     to_pair.wait()
     small_y[cy] = small[pl.ds(par * half, half)] + small_in[...]
@@ -371,7 +371,6 @@
         small_y_copy(i).start()
     y_stage(zsize - 1)
 
-    gated_gradient(0)
     for k in range(2, zsize - 1):
         z_stage(k)
     gated_gradient(1)

time: 41.1 us -> 41.3 us (level)
  no operation moved by 1% of the time
where the time goes in v4:
time: 41.3 us; the launch traced here: 41.1 us
  Pallas kernels  40.5 us (98%)
  between operations  0.64 us (2%)
    pallas_call x1, Pallas kernels, on_device(): pl.pallas_call(functools.partial(kernel, n, tp, taps_n, ysize), out_shape...  39.3 us
    pallas_call x1, Pallas kernels, on_device(): pl.pallas_call(write_out, out_shape=[jax.ShapeDtypeStruct(r.shape, r.dtyp...  1.12 us

profile of v4, /device:TPU:0, one launch (start us, length us, event | category | flops | bytes accessed | tf_op | source)
XLA Modules:
  0.0 41.1 jit_solution(16673048609799064667)
XLA Ops:
  0.6 39.3 %shard_map.118 = (bf16[512,512]{1,0:T(8,128)(2,1)S(1)}, bf16[512,512]{1,0:T(8,128)(2,1)S(1)}, f32[128,512]{1,0:T(8,128)S(1)}, f32[31,512]{1,0:T(8,128)S(1)}, f32[1,512]{1,0:T(1,128)S(1)}, /*index=5*/f32[1,512]{1,0:T(1,128)S(1)}) custom-call(bf16[512,512]{1,0:T(8,128)(2,1)} %value_hbm.1, bf16[512,512]{1,0:T(8,128)(2,1)} %gate_hbm.1, f32[31,512]{1,0:T(8,128)} %taps_hbm.1, ...), custom_call_target="tpu_custom_call" | custom-call | tf_op jit(solution)/shard_map/pallas_call | solution.py:452
  40.0 1.1 %shard_map.119 = (bf16[512,512]{1,0:T(8,128)(2,1)}, bf16[512,512]{1,0:T(8,128)(2,1)}, f32[128,512]{1,0:T(8,128)}, f32[31,512]{1,0:T(8,128)}, f32[1,512]{1,0:T(1,128)}, /*index=5*/f32[1,512]{1,0:T(1,128)}) custom-call(bf16[512,512]{1,0:T(8,128)(2,1)S(1)} %get-tuple-element.18.refs_0_, bf16[512,512]{1,0:T(8,128)(2,1)S(1)} %get-tuple-element.19.refs_1_, ...), custom_call_target="tpu_custom_call" | custom-call | tf_op jit(solution)/shard_map/pallas_call | solution.py:518
